TPU v7x, 512 devices: a whole 4x4x16 slice. The times are simulated.
512 devices in a mesh: sp: 32 (over z, core), tp: 16 (over y, x).
Axes of the slice: x: 4, y: 4, z: 16, core: 2. Of those that a mesh axis runs over, the one named last changes fastest.
Arguments:
- residual: bfloat16 [4096, 4096], P('sp', 'tp'), may hold values from -46 to 46
- query_small: bfloat16 [4096, 2048], P('sp', 'tp'), may hold values from -6 to 6
- key_narrow_group: bfloat16 [4096, 2048], P('sp', 'tp'), may hold values from -6 to 6
- query_large: bfloat16 [4096, 4096], P('sp', 'tp'), may hold values from -6 to 6
- key_large: bfloat16 [4096, 4096], P('sp', 'tp'), may hold values from -6 to 6
- values: bfloat16 [4096, 2, 2048], P('sp', None, 'tp'), may hold values from -6 to 6
- gates: bfloat16 [4096, 2, 2048], P('sp', None, 'tp'), may hold values from -6 to 6
- log_decay: float32 [4096, 2, 16], P('sp', None, 'tp'), may hold values from -0.65 to 0, as said below
- head_gain: float32 [2, 2048], P(None, 'tp'), may hold values from 0.1 to 1.9
- out_weight: bfloat16 [2, 2048, 4096], P(None, 'sp', 'tp'), may hold values from -0.09375 to 0.09375
- norm_gain: float32 [4096], P('tp'), may hold values from 0.1 to 1.9
- routes: int32 [4096, 2], P('sp'), may hold values from 0 to 31, all different within a row; in each aligned block of 128 rows (0 to 127, 128 to 255, ...) at most 16 rows name the same one
- route_weight: float32 [4096, 2], P('sp'), may hold values from 0.2 to 1
- expert_gate: bfloat16 [32, 4096, 2048], P('sp', None, 'tp'), may hold values from -0.09375 to 0.09375
- expert_up: bfloat16 [32, 4096, 2048], P('sp', None, 'tp'), may hold values from -0.09375 to 0.09375
- expert_down: bfloat16 [32, 2048, 4096], P('sp', None, 'tp'), may hold values from -0.5 to 0.5
Outputs:
- new_stream: bfloat16 [4096, 4096], P('sp', 'tp')
Inputs may be any that keep to these rules, and one draw needn't show every extreme that they name: `routes`: each row names two different experts; in each aligned block of 128 rows no expert is named more than 16 times, a bound that some block reaches. `log_decay`: negative at every position.
All inputs are finite; a program needn't handle non-finite values.
Results may differ from a plain program's by a relative error of at most 0.019.
Values may be sent and summed in bfloat16 or wider, within the bound.
A program may use at most 64 MiB of HBM per device.

v0:
```python
import functools
import jax
import jax.numpy as jnp
from jax import lax
from jax.sharding import Mesh
from jax.sharding import PartitionSpec as P

D = 4096
SP = ("sp_0", "sp_1")
TP = ("tp_0", "tp_1")
EPS = 1e-06
THETA = 10000.0


def neutral_like(array, identity):
    return jax.tree.map(
        lambda a, e: jnp.broadcast_to(jnp.asarray(e, a.dtype), a.shape), array, identity
    )


def gathered_once(array, axis):
    leaves = jax.tree.leaves(array)
    order = sorted(range(len(leaves)), key=lambda k: -leaves[k].size)
    width = (1, *leaves[order[0]].shape)[-1]
    lines = [
        jnp.pad(leaves[k].reshape(-1), (0, -leaves[k].size % width)).reshape(-1, width)
        for k in order
    ]
    both, at, found = (lax.all_gather(jnp.concatenate(lines), axis), 0, {})
    for k, line in zip(order, lines):
        piece = both[:, at : at + len(line)].reshape(len(both), -1)
        found[k] = piece[:, : leaves[k].size].reshape(-1, *leaves[k].shape)
        at += len(line)
    numbers = iter(range(len(leaves)))
    return jax.tree.map(lambda _: found[next(numbers)], array)


def entering_2(array, axes, combine, identity):
    before = start = neutral_like(array, identity)
    so_far = array
    for axis in reversed(axes):
        devices, place = (lax.axis_size(axis), lax.axis_index(axis))
        pieces = gathered_once(so_far, axis)
        inside, so_far = (start, start)
        for k in range(devices):
            passed = k < place
            so_far = combine(so_far, jax.tree.map(lambda part: part[k], pieces))
            inside = jax.tree.map(lambda new, old: jnp.where(passed, new, old), so_far, inside)
        before = combine(inside, before)
    return before


def in_order(blocks, dim):
    lengths = list(blocks.shape[1:])
    lengths[dim] *= blocks.shape[0]
    return jnp.moveaxis(blocks, 0, dim).reshape(lengths)


def from_everyone(array, axis):
    devices = lax.axis_size(axis)
    return lax.all_to_all(
        jnp.broadcast_to(array[None], (devices, *array.shape)), axis, 0, 0, tiled=True
    )


def gathered_copies(array, axis, dim):
    return in_order(from_everyone(array, axis), dim)


def by_axis(array, axes):
    return functools.reduce(lax.psum, axes, array)


def rotate(block, positions):
    half_dim = block.shape[-1] // 2
    inverse = jnp.power(THETA, -jnp.arange(half_dim, dtype=jnp.float32) * 2.0 / block.shape[-1])
    angles = positions[:, None, None] * inverse
    cosine_val, sine_val = (jnp.cos(angles), jnp.sin(angles))
    lower_half, upper_half = (block[..., :half_dim], block[..., half_dim:])
    return jnp.concatenate(
        [
            lower_half * cosine_val - upper_half * sine_val,
            upper_half * cosine_val + lower_half * sine_val,
        ],
        axis=-1,
    )


def block_terms(rot_queries, rot_keys, value_heads, rates):
    count = rates.shape[0]
    decay_sum = jnp.cumsum(rates, axis=0)
    by_head = decay_sum.T
    causal = (jnp.arange(count)[:, None] >= jnp.arange(count)[None, :])[None]
    spread = by_head[:, :, None] - by_head[:, None, :]
    weight = jnp.where(causal, jnp.exp(jnp.where(causal, spread, 0.0)), 0.0)
    scores = jnp.einsum("ihd,jhd->hij", rot_queries, rot_keys, preferred_element_type=jnp.float32)
    weighted = (scores * weight).astype(jnp.bfloat16)
    within = jnp.einsum("hij,jhv->ihv", weighted, value_heads, preferred_element_type=jnp.float32)
    block_end = decay_sum[-1]
    carried = (
        rot_keys.astype(jnp.float32) * jnp.exp(block_end[None, :] - decay_sum)[:, :, None]
    ).astype(jnp.bfloat16)
    update = jnp.einsum("jhd,jhv->hdv", carried, value_heads, preferred_element_type=jnp.float32)
    return (within, decay_sum, jnp.exp(block_end), update)


def final_result(rot_queries, decay_sum, within, state_in, gate_part, gain_part):
    cross_part = (
        jnp.einsum(
            "ihd,hdv->ihv",
            rot_queries.astype(jnp.float32),
            state_in,
            precision=lax.Precision.HIGHEST,
        )
        * jnp.exp(decay_sum)[:, :, None]
    )
    retained = within + cross_part
    scaled = retained * lax.rsqrt(jnp.mean(retained * retained, axis=-1, keepdims=True) + EPS)
    count, head_count, value_size = retained.shape
    gated = jax.nn.silu(gate_part.astype(jnp.float32)).reshape(count, head_count, value_size)
    return (
        (scaled * gain_part.reshape(head_count, value_size) * gated)
        .reshape(count, -1)
        .astype(jnp.bfloat16)
    )


def prepare(queries, keys_in, value_part, positions, head_count):
    row_count = queries.shape[0]
    key_size = queries.shape[1] // head_count
    rot_queries = rotate(
        queries.astype(jnp.float32).reshape(row_count, head_count, key_size), positions
    ).astype(jnp.bfloat16)
    rot_keys = (
        rotate(keys_in.astype(jnp.float32).reshape(row_count, head_count, key_size), positions)
        * key_size ** (-0.5)
    ).astype(jnp.bfloat16)
    value_heads = value_part.reshape(row_count, head_count, value_part.shape[1] // head_count)
    return (rot_queries, rot_keys, value_heads)


def per_device(
    residual,
    query_small,
    key_narrow_group,
    query_large,
    key_large,
    values,
    gates,
    log_decay,
    head_gain,
    out_weight,
    norm_gain,
    routes,
    route_weight,
    expert_gate,
    expert_up,
    expert_down,
):
    row_count = residual.shape[0]
    head_count = log_decay.shape[2]
    positions = (lax.axis_index(SP) * row_count + jnp.arange(row_count, dtype=jnp.int32)).astype(
        jnp.float32
    )
    query_a, key_a, value_a = prepare(
        query_small, key_narrow_group, values[:, 0], positions, head_count
    )
    query_b, key_b, value_b = prepare(query_large, key_large, values[:, 1], positions, head_count)
    within_a, decay_sum_a, fall_a, update_a = block_terms(query_a, key_a, value_a, log_decay[:, 0])
    within_b, decay_sum_b, fall_b, update_b = block_terms(query_b, key_b, value_b, log_decay[:, 1])

    def combine(before_part, after_part):
        return (
            before_part[0] * after_part[0],
            after_part[0][:, None, None] * before_part[1] + after_part[1],
            before_part[2] * after_part[2],
            after_part[2][:, None, None] * before_part[3] + after_part[3],
        )

    identity = (
        jnp.ones_like(fall_a),
        jnp.zeros_like(update_a),
        jnp.ones_like(fall_b),
        jnp.zeros_like(update_b),
    )
    entering = entering_2((fall_a, update_a, fall_b, update_b), SP, combine, identity)
    output_a = final_result(query_a, decay_sum_a, within_a, entering[1], gates[:, 0], head_gain[0])
    output_b = final_result(query_b, decay_sum_b, within_b, entering[3], gates[:, 1], head_gain[1])
    stacked = jnp.stack([output_a, output_b], axis=1)
    gathered = gathered_copies(stacked, TP, 2)
    mixed = jnp.einsum(
        "tgk,gkd->td",
        gathered,
        lax.all_gather(out_weight, SP, axis=1, tiled=True),
        preferred_element_type=jnp.float32,
    ).astype(jnp.bfloat16)
    stream = residual.astype(jnp.float32) + mixed.astype(jnp.float32)
    square_sum = by_axis(jnp.sum(stream * stream, axis=1), TP)
    normed = (stream * lax.rsqrt(square_sum / D + EPS)[:, None] * norm_gain[None, :]).astype(
        jnp.bfloat16
    )
    experts = lax.axis_size(SP)
    capacity = 4 * row_count // experts
    one_hot = (routes[:, :, None] == jnp.arange(experts, dtype=jnp.int32)[None, None, :]).astype(
        jnp.int32
    )
    one_hot = one_hot.reshape(2 * row_count, experts)
    before = jnp.cumsum(one_hot, axis=0) - one_hot
    slot_index = jnp.sum(before * one_hot, axis=1).reshape(row_count, 2)
    target = routes * capacity + slot_index
    slot_ids = jnp.arange(experts * capacity, dtype=jnp.int32)
    choose = target[:, :, None] == slot_ids[None, None, :]
    select = jnp.sum(choose.astype(jnp.int32), axis=1).astype(jnp.bfloat16).T
    w_gate, w_up, w_down = (expert_gate[0], expert_up[0], expert_down[0])
    outgoing = jnp.dot(select, normed, preferred_element_type=jnp.float32).astype(jnp.bfloat16)
    outgoing = outgoing.reshape(experts, capacity, normed.shape[1])
    arrived = lax.all_to_all(outgoing, SP, split_axis=0, concat_axis=0, tiled=True)
    expert_arrived = lax.all_gather(arrived, TP, axis=2, tiled=True)
    gate_part = jnp.einsum(
        "sck,kf->scf", expert_arrived, w_gate, preferred_element_type=jnp.float32
    )
    up_part = jnp.einsum("sck,kf->scf", expert_arrived, w_up, preferred_element_type=jnp.float32)
    hidden = (jax.nn.silu(gate_part) * up_part).astype(jnp.bfloat16)
    expert_out = jnp.einsum(
        "scf,fd->scd", gathered_copies(hidden, TP, 2), w_down, preferred_element_type=jnp.float32
    ).astype(jnp.bfloat16)
    returned = lax.all_to_all(expert_out, SP, split_axis=0, concat_axis=0, tiled=True).reshape(
        experts * capacity, -1
    )
    first_pick = jnp.dot(
        choose[:, 0].astype(jnp.bfloat16), returned, preferred_element_type=jnp.float32
    )
    second_pick = jnp.dot(
        choose[:, 1].astype(jnp.bfloat16), returned, preferred_element_type=jnp.float32
    )
    routed = route_weight[:, 0:1] * first_pick + route_weight[:, 1:2] * second_pick
    return (stream + routed).astype(jnp.bfloat16)


def solution(mesh):
    torus = Mesh(mesh.devices.reshape(16, 2, 4, 4), ("sp_0", "sp_1", "tp_0", "tp_1"))
    placed = (
        P(SP, TP),
        P(SP, TP),
        P(SP, TP),
        P(SP, TP),
        P(SP, TP),
        P(SP, None, TP),
        P(SP, None, TP),
        P(SP, None, TP),
        P(None, TP),
        P(None, SP, TP),
        P(TP),
        P(SP, None),
        P(SP, None),
        P(SP, None, TP),
        P(SP, None, TP),
        P(SP, None, TP),
    )
    return jax.shard_map(
        per_device, mesh=torus, in_specs=placed, out_specs=P(SP, TP), check_vma=False
    )
```

profile of v0, /device:TPU:1, one launch (start us, length us, event | category | flops | bytes accessed | tf_op | source)
XLA Modules:
  0.0 372.4 jit_solution(16960491022823976062)
XLA Ops:
  6.6 0.8 slice_bitcast_fusion.9
  9.3 1.0 fusion.295
  11.7 0.9 bitcast_convert_fusion
  13.2 0.8 bitcast_convert_fusion.2
  15.9 8.6 %all-gather.2 = f32[2,386,128]{2,1,0:T(8,128)S(1)} all-gather(f32[1,386,128]{2,1,0:T(8,128)S(1)} %maximum_bitcast_fusion), channel_id=2, replica_groups=mesh['sp_0'=16,'sp_1'=2,'tp_0'=4,'tp_1'=4] {'sp_1'}, dimensions={0}, use_global_device_ids=true | all-gather | bytes 592896 | tf_op jit(solution)/shard_map/all_gather | solution.py:29
  34.0 63.0 %all-gather.12.cloned.1.call-done = f32[16,386,128]{2,1,0:T(8,128)} async-done(((f32[1,386,128]{2,1,0:T(8,128)}), f32[16,386,128]{2,1,0:T(8,128)}) %all-gather.12.cloned.1.call-update) | async-done | bytes 3162128 | tf_op jit(solution)/shard_map/all_gather | solution.py:29
  97.0 0.9 fusion.292
  100.4 11.6 %fusion.16 = f32[1,128,128]{2,1,0:T(8,128)S(1)} fusion(f32[16,386,128]{2,1,0:T(8,128)} %all-gather.12.cloned.1.call-done, f32[2,386,128]{2,1,0:T(8,128)S(1)} %all-gather.2, f32[128]{0:T(128)S(1)} %get-tuple-element.71, f32[]{:T(128)} %bitcast.63, f32[]{:T(128)} %bitcast.62, f32[]{:T(128)} %bitcast.61, f32[]{:T(128)} %bitcast.60, f32[]{:T(128)} %bitcast.59, ...), kind=kOutput, calls=%fused_computation.25 | convolution fusion | flops 26132480 | bytes 1322000 | tf_op jit(solution)/shard_map/ihd,hdv->ihv/dot_general | solution.py:109
  112.3 12.2 %multiply_reduce_fusion.1 = (f32[128]{0:T(128)S(1)}, f32[1,128,128]{2,1,0:T(8,128)S(1)}) fusion(f32[1,128,128]{2,1,0:T(8,128)S(1)} %convolution_bitcast_fusion.2, f32[128]{0:T(128)S(1)} %get-tuple-element.73, bf16[128,128]{1,0:T(8,128)(2,1)S(1)} %get-tuple-element.67, bf16[128,128]{1,0:T(8,128)(2,1)S(1)} %get-tuple-element.68, ...), kind=kOutput, calls=%fused_computation.180 | convolution fusion | flops 52297600 | bytes 2567696 | tf_op jit(solution)/shard_map/ihd,hdv->ihv/dot_general | solution.py:109
  124.9 1.2 broadcast_in_dim.18
  126.1 6.7 %all-to-all-start = ((bf16[16,128,2,128]{3,1,2,0:T(8,128)(2,1)}), bf16[16,128,2,128]{3,1,2,0:T(8,128)(2,1)S(1)}, u32[]{:S(2)}, u32[]{:S(2)}) async-start(bf16[16,128,2,128]{3,1,2,0:T(8,128)(2,1)} %broadcast_in_dim.18), calls=%async_computation | async-start | bytes 2097152 | tf_op jit(solution)/shard_map/all_to_all | solution.py:61
  134.5 42.4 %all-gather.8.cloned.1.call-done = bf16[2,2048,256]{2,1,0:T(8,128)(2,1)} async-done(((bf16[2,64,256]{2,1,0:T(8,128)(2,1)}), bf16[2,2048,256]{2,1,0:T(8,128)(2,1)}) %all-gather.8.cloned.1.call-update) | async-done | bytes 2097168 | tf_op jit(solution)/shard_map/all_gather | solution.py:194
  177.0 2.2 multiply_reduce_fusion
  179.1 8.3 %psum.14 = f32[128]{0:T(128)S(1)} all-reduce(f32[128]{0:T(128)S(1)} %get-tuple-element.79), channel_id=1, replica_groups=mesh['sp_0'=16,'sp_1'=2,'tp_0'=4,'tp_1'=4] {'tp_0'}, use_global_device_ids=true, to_apply=%region_9.10 | all-reduce | flops 128 | bytes 1024 | tf_op jit(solution)/shard_map/psum | solution.py:71
  187.4 8.4 %psum.15 = f32[128]{0:T(128)S(1)} all-reduce(f32[128]{0:T(128)S(1)} %psum.14), channel_id=1, replica_groups=mesh['sp_0'=16,'sp_1'=2,'tp_0'=4,'tp_1'=4] {'tp_1'}, use_global_device_ids=true, to_apply=%region_10.11 | all-reduce | flops 128 | bytes 1024 | tf_op jit(solution)/shard_map/psum | solution.py:71
  196.2 34.8 %all_to_all.20 = bf16[32,16,256]{2,1,0:T(8,128)(2,1)} all-to-all(bf16[32,16,256]{2,1,0:T(8,128)(2,1)S(1)} %bitcast.244), channel_id=1, replica_groups=mesh['sp_0'=16,'sp_1'=2,'tp_0'=4,'tp_1'=4] {'sp_0','sp_1'}, dimensions={0} | all-to-all | bytes 524288 | tf_op jit(solution)/shard_map/all_to_all | solution.py:217
  231.0 57.7 %all-gather.10.cloned.1.call-done = bf16[32,16,4096]{2,1,0:T(8,128)(2,1)} async-done(((bf16[32,16,256]{2,1,0:T(8,128)(2,1)}), bf16[32,16,4096]{2,1,0:T(8,128)(2,1)}) %all-gather.10.cloned.1.call-update) | async-done | bytes 4194320 | tf_op jit(solution)/shard_map/all_gather | solution.py:218
  288.7 3.6 fusion.23
  292.3 1.3 fusion.6
  294.0 31.7 %all_to_all.21 = bf16[16,32,16,128]{3,2,1,0:T(8,128)(2,1)S(1)} all-to-all(bf16[16,32,16,128]{3,2,1,0:T(8,128)(2,1)S(1)} %broadcast_in_dim.19), channel_id=1, replica_groups=mesh['sp_0'=16,'sp_1'=2,'tp_0'=4,'tp_1'=4] {'tp_0','tp_1'}, dimensions={0} | all-to-all | bytes 4194304 | tf_op jit(solution)/shard_map/all_to_all | solution.py:61
  325.7 1.4 fusion.3
  327.1 15.5 %all-to-all-start.3 = ((bf16[32,16,256]{2,1,0:T(8,128)(2,1)}), bf16[32,16,256]{2,1,0:T(8,128)(2,1)S(1)}, u32[]{:S(2)}, u32[]{:S(2)}) async-start(bf16[32,16,256]{2,1,0:T(8,128)(2,1)} %fusion.3), calls=%async_computation.3 | async-start | bytes 524288 | tf_op jit(solution)/shard_map/all_to_all | solution.py:227
  342.7 22.1 %all-to-all-done.3 = bf16[32,16,256]{2,1,0:T(8,128)(2,1)S(1)} async-done(((bf16[32,16,256]{2,1,0:T(8,128)(2,1)}), bf16[32,16,256]{2,1,0:T(8,128)(2,1)S(1)}, u32[]{:S(2)}, u32[]{:S(2)}) %all-to-all-start.3) | async-done | bytes 262176 | tf_op jit(solution)/shard_map/all_to_all | solution.py:227
  365.0 0.8 fusion.9
  (85 shorter events, 13.8 us)
Async XLA Ops:
  6.5 319.1 %copy-start = (bf16[1,2048,256]{2,1,0:T(8,128)(2,1)S(1)}, bf16[1,2048,256]{2,1,0:T(8,128)(2,1)}, u32[]{:S(2)}) copy-start(bf16[1,2048,256]{2,1,0:T(8,128)(2,1)} %param.31) | copy-start | bytes 3145732
  6.5 26.7 %copy-start.3 = (bf16[128,2,128]{2,1,0:T(2,128)(2,1)S(1)}, bf16[128,2,128]{2,1,0:T(2,128)(2,1)}, u32[]{:S(2)}) copy-start(bf16[128,2,128]{2,1,0:T(2,128)(2,1)} %param.22) | copy-start | bytes 196612
  6.5 27.4 %copy-start.6 = (f32[2,128]{1,0:T(2,128)S(1)}, f32[2,128]{1,0:T(2,128)}, u32[]{:S(2)}) copy-start(f32[2,128]{1,0:T(2,128)} %param.24) | copy-start | bytes 3076
  6.5 90.4 %all-gather.12.cloned.1.call-start = ((), (), s32[]{:S(2)}) async-start(), calls=%async_computation.6 | async-start | bytes 3411968 | tf_op jit(solution)/shard_map/all_gather | solution.py:29
  31.3 145.7 %all-gather.8.cloned.1.call-start = ((), (), s32[]{:S(2)}) async-start(), calls=%async_computation.4 | async-start | bytes 2162688 | tf_op jit(solution)/shard_map/all_gather | solution.py:194
  112.3 20.5 %copy-start.4 = (s32[128,2]{0,1:T(2,128)S(1)}, s32[128,2]{0,1:T(2,128)}, u32[]{:S(2)}) copy-start(s32[128,2]{0,1:T(2,128)} %param.27) | copy-start | bytes 3076
  126.1 69.8 %copy-start.5 = (f32[256]{0:T(256)S(1)}, f32[256]{0:T(256)}, u32[]{:S(2)}) copy-start(f32[256]{0:T(256)} %param.26) | copy-start | bytes 3076
  126.1 50.8 %all-to-all-start = ((bf16[16,128,2,128]{3,1,2,0:T(8,128)(2,1)}), bf16[16,128,2,128]{3,1,2,0:T(8,128)(2,1)S(1)}, u32[]{:S(2)}, u32[]{:S(2)}) async-start(bf16[16,128,2,128]{3,1,2,0:T(8,128)(2,1)} %broadcast_in_dim.18), calls=%async_computation | async-start | bytes 2097152 | tf_op jit(solution)/shard_map/all_to_all | solution.py:61
  132.8 155.9 %copy-start.2 = (bf16[1,4096,128]{2,1,0:T(8,128)(2,1)S(1)}, bf16[1,4096,128]{2,1,0:T(8,128)(2,1)}, u32[]{:S(2)}) copy-start(bf16[1,4096,128]{2,1,0:T(8,128)(2,1)} %param.29) | copy-start | bytes 3145732
  132.8 155.9 %all-gather.10.cloned.1.call-start = ((), (), s32[]{:S(2)}) async-start(), calls=%async_computation.5 | async-start | bytes 4456448 | tf_op jit(solution)/shard_map/all_gather | solution.py:218
  196.2 96.1 %copy-start.8 = (bf16[1,4096,128]{2,1,0:T(8,128)(2,1)S(1)}, bf16[1,4096,128]{2,1,0:T(8,128)(2,1)}, u32[]{:S(2)}) copy-start(bf16[1,4096,128]{2,1,0:T(8,128)(2,1)} %param.30) | copy-start | bytes 3145732
  288.7 3.6 copy-start.1
  325.7 16.9 %copy-start.7 = (f32[128,2]{0,1:T(2,128)S(1)}, f32[128,2]{0,1:T(2,128)}, u32[]{:S(2)}) copy-start(f32[128,2]{0,1:T(2,128)} %param.28) | copy-start | bytes 3076
  327.1 37.7 %all-to-all-start.3 = ((bf16[32,16,256]{2,1,0:T(8,128)(2,1)}), bf16[32,16,256]{2,1,0:T(8,128)(2,1)S(1)}, u32[]{:S(2)}, u32[]{:S(2)}) async-start(bf16[32,16,256]{2,1,0:T(8,128)(2,1)} %fusion.3), calls=%async_computation.3 | async-start | bytes 524288 | tf_op jit(solution)/shard_map/all_to_all | solution.py:227
Sparse Core Ops, SparseCore 0:
  31.4 65.5 all-gather.11
  99.1 77.7 all-gather.7
  231.1 57.5 all-gather.9
where the time goes:
time: 374 us; the launch traced here: 372 us
  waiting for transfers between devices  186 us (50%)
  blocking collectives  91.8 us (25%)
  matrix products  34.7 us (9%)
  starting transfers between devices  22.2 us (6%)
  between operations  20.9 us (6%)
  local copies, waits for them, and re-layouts  9.36 us (3%)
  other arithmetic  7.46 us (2%)
    all_gather x1, waiting for transfers between devices, gathered_once(): both, at, found = (lax.all_gather(jnp.concatenate(lines), axis), 0, {})  63 us
    all_gather x1, waiting for transfers between devices, per_device(): expert_arrived = lax.all_gather(arrived, TP, axis=2, tiled=True)  57.7 us
    all_gather x1, waiting for transfers between devices, per_device(): lax.all_gather(out_weight, SP, axis=1, tiled=True)  42.4 us
    all_to_all x1, blocking collectives, per_device(): lax.all_to_all(outgoing, SP, split_axis=0, concat_axis=0, tiled=True)  34.8 us
    all_to_all x1, blocking collectives, from_everyone(): lax.all_to_all(jnp.broadcast_to(array[None], (devices, *array.shape)), ax...  31.7 us
    dot_general x2, matrix products, final_result(): jnp.einsum('ihd,hdv->ihv', rot_queries.astype(jnp.float32), state_in, pre...  23.7 us
    all_to_all x1, waiting for transfers between devices, per_device(): lax.all_to_all(expert_out, SP, split_axis=0, concat_axis=0, tiled=True)  22.1 us
    psum x2, blocking collectives, by_axis(): return functools.reduce(lax.psum, axes, array)  16.8 us
  transfers between devices with their start and end apart: 5, of which 4 were waited for; matrix products, arithmetic and copies ran while one was open for 8% of the time, Pallas kernels for 0%

commit v1 on v0

--- a/solution.py
+++ b/solution.py
@@ -4,6 +4,7 @@
 from jax import lax
 from jax.sharding import Mesh
 from jax.sharding import PartitionSpec as P
+from jax.lax import all_to_all, axis_size
 
 D = 4096
 SP = ("sp_0", "sp_1")
@@ -215,7 +216,12 @@
     outgoing = jnp.dot(select, normed, preferred_element_type=jnp.float32).astype(jnp.bfloat16)
     outgoing = outgoing.reshape(experts, capacity, normed.shape[1])
     arrived = lax.all_to_all(outgoing, SP, split_axis=0, concat_axis=0, tiled=True)
-    expert_arrived = lax.all_gather(arrived, TP, axis=2, tiled=True)
+    expert_arrived = jnp.concatenate(
+        all_to_all(
+            jnp.stack([arrived for _ in range(axis_size(TP))]), TP, split_axis=0, concat_axis=0
+        ),
+        axis=2,
+    )
     gate_part = jnp.einsum(
         "sck,kf->scf", expert_arrived, w_gate, preferred_element_type=jnp.float32
     )

time: 374 us -> 358 us (0.957)
  waiting for transfers between devices: 186 us -> 128 us
  blocking collectives: 91.8 us -> 143 us
  starting transfers between devices: 22.2 us -> 13.9 us
    all_gather x1 -> x0, waiting for transfers between devices: 57.7 us -> none  [per_device(): expert_arrived = lax.all_gather(arrived, TP, axis=2, tiled=True)]
    all_to_all x0 -> x1, blocking collectives: none -> 52.7 us  [per_device(): all_to_all(jnp.stack([arrived for _ in range(axis_size(TP))]), TP, split_...]
    all_to_all x1, starting transfers between devices: 15.5 us -> 7.24 us  [per_device(): lax.all_to_all(expert_out, SP, split_axis=0, concat_axis=0, tiled=True)]
  transfers between devices with their start and end apart: 5 -> 4, of which waited for: 4 -> 3; matrix products, arithmetic and copies ran while one was open for 8% -> 9% of each run, Pallas kernels for 0% -> 0%
where the time goes in v1:
time: 358 us; the launch traced here: 357 us
  blocking collectives  143 us (40%)
  waiting for transfers between devices  128 us (36%)
  matrix products  32.3 us (9%)
  between operations  21.5 us (6%)
  starting transfers between devices  13.9 us (4%)
  local copies, waits for them, and re-layouts  10.9 us (3%)
  other arithmetic  7.34 us (2%)
    all_gather x1, waiting for transfers between devices, gathered_once(): both, at, found = (lax.all_gather(jnp.concatenate(lines), axis), 0, {})  62.9 us
    all_to_all x1, blocking collectives, per_device(): all_to_all(jnp.stack([arrived for _ in range(axis_size(TP))]), TP, split_...  52.7 us
    all_gather x1, waiting for transfers between devices, per_device(): lax.all_gather(out_weight, SP, axis=1, tiled=True)  42.4 us
    all_to_all x1, blocking collectives, per_device(): lax.all_to_all(outgoing, SP, split_axis=0, concat_axis=0, tiled=True)  34.3 us
    all_to_all x1, blocking collectives, from_everyone(): lax.all_to_all(jnp.broadcast_to(array[None], (devices, *array.shape)), ax...  30.3 us
    dot_general x2, matrix products, final_result(): jnp.einsum('ihd,hdv->ihv', rot_queries.astype(jnp.float32), state_in, pre...  23.7 us
    all_to_all x1, waiting for transfers between devices, per_device(): lax.all_to_all(expert_out, SP, split_axis=0, concat_axis=0, tiled=True)  22.1 us
    psum x2, blocking collectives, by_axis(): return functools.reduce(lax.psum, axes, array)  16.7 us
  transfers between devices with their start and end apart: 4, of which 3 were waited for; matrix products, arithmetic and copies ran while one was open for 9% of the time, Pallas kernels for 0%

profile of v1, /device:TPU:1, one launch (start us, length us, event | category | flops | bytes accessed | tf_op | source)
XLA Modules:
  0.0 356.8 jit_solution(840058625906911837)
XLA Ops:
  6.6 0.8 slice_bitcast_fusion.9
  9.2 1.0 fusion.295
  11.5 0.9 bitcast_convert_fusion
  13.1 0.8 bitcast_convert_fusion.2
  15.7 8.6 %all-gather.2 = f32[2,386,128]{2,1,0:T(8,128)S(1)} all-gather(f32[1,386,128]{2,1,0:T(8,128)S(1)} %maximum_bitcast_fusion), channel_id=2, replica_groups=mesh['sp_0'=16,'sp_1'=2,'tp_0'=4,'tp_1'=4] {'sp_1'}, dimensions={0}, use_global_device_ids=true | all-gather | bytes 592896 | tf_op jit(solution)/shard_map/all_gather | solution.py:30
  34.0 62.9 %all-gather.9.cloned.1.call-done = f32[16,386,128]{2,1,0:T(8,128)} async-done(((f32[1,386,128]{2,1,0:T(8,128)}), f32[16,386,128]{2,1,0:T(8,128)}) %all-gather.9.cloned.1.call-update) | async-done | bytes 3162128 | tf_op jit(solution)/shard_map/all_gather | solution.py:30
  96.9 0.9 fusion.292
  100.4 11.5 %fusion.16 = f32[1,128,128]{2,1,0:T(8,128)S(1)} fusion(f32[16,386,128]{2,1,0:T(8,128)} %all-gather.9.cloned.1.call-done, f32[2,386,128]{2,1,0:T(8,128)S(1)} %all-gather.2, f32[128]{0:T(128)S(1)} %get-tuple-element.71, f32[]{:T(128)} %bitcast.63, f32[]{:T(128)} %bitcast.62, f32[]{:T(128)} %bitcast.61, f32[]{:T(128)} %bitcast.60, f32[]{:T(128)} %bitcast.59, ...), kind=kOutput, calls=%fused_computation.25 | convolution fusion | flops 26132480 | bytes 1322000 | tf_op jit(solution)/shard_map/ihd,hdv->ihv/dot_general | solution.py:110
  112.4 12.2 %multiply_reduce_fusion.1 = (f32[128]{0:T(128)S(1)}, f32[1,128,128]{2,1,0:T(8,128)S(1)}) fusion(f32[1,128,128]{2,1,0:T(8,128)S(1)} %convolution_bitcast_fusion.2, f32[128]{0:T(128)S(1)} %get-tuple-element.73, bf16[128,128]{1,0:T(8,128)(2,1)S(1)} %get-tuple-element.67, bf16[128,128]{1,0:T(8,128)(2,1)S(1)} %get-tuple-element.68, ...), kind=kOutput, calls=%fused_computation.180 | convolution fusion | flops 52297600 | bytes 2567696 | tf_op jit(solution)/shard_map/ihd,hdv->ihv/dot_general | solution.py:110
  124.9 1.2 broadcast_in_dim.18
  126.1 6.7 %all-to-all-start = ((bf16[16,128,2,128]{3,1,2,0:T(8,128)(2,1)}), bf16[16,128,2,128]{3,1,2,0:T(8,128)(2,1)S(1)}, u32[]{:S(2)}, u32[]{:S(2)}) async-start(bf16[16,128,2,128]{3,1,2,0:T(8,128)(2,1)} %broadcast_in_dim.18), calls=%async_computation | async-start | bytes 2097152 | tf_op jit(solution)/shard_map/all_to_all | solution.py:62
  134.5 42.4 %all-gather.7.cloned.1.call-done = bf16[2,2048,256]{2,1,0:T(8,128)(2,1)} async-done(((bf16[2,64,256]{2,1,0:T(8,128)(2,1)}), bf16[2,2048,256]{2,1,0:T(8,128)(2,1)}) %all-gather.7.cloned.1.call-update) | async-done | bytes 2097168 | tf_op jit(solution)/shard_map/all_gather | solution.py:195
  176.9 2.1 multiply_reduce_fusion
  179.1 8.3 %psum.14 = f32[128]{0:T(128)S(1)} all-reduce(f32[128]{0:T(128)S(1)} %get-tuple-element.79), channel_id=1, replica_groups=mesh['sp_0'=16,'sp_1'=2,'tp_0'=4,'tp_1'=4] {'tp_0'}, use_global_device_ids=true, to_apply=%region_9.10 | all-reduce | flops 128 | bytes 1024 | tf_op jit(solution)/shard_map/psum | solution.py:72
  187.3 8.5 %psum.15 = f32[128]{0:T(128)S(1)} all-reduce(f32[128]{0:T(128)S(1)} %psum.14), channel_id=1, replica_groups=mesh['sp_0'=16,'sp_1'=2,'tp_0'=4,'tp_1'=4] {'tp_1'}, use_global_device_ids=true, to_apply=%region_10.11 | all-reduce | flops 128 | bytes 1024 | tf_op jit(solution)/shard_map/psum | solution.py:72
  196.1 34.3 %all_to_all.25 = bf16[32,16,256]{2,1,0:T(8,128)(2,1)S(1)} all-to-all(bf16[32,16,256]{2,1,0:T(8,128)(2,1)S(1)} %bitcast.250), channel_id=1, replica_groups=mesh['sp_0'=16,'sp_1'=2,'tp_0'=4,'tp_1'=4] {'sp_0','sp_1'}, dimensions={0} | all-to-all | bytes 524288 | tf_op jit(solution)/shard_map/all_to_all | solution.py:218
  230.8 52.7 %all_to_all.26 = bf16[16,32,16,256]{3,2,1,0:T(8,128)(2,1)S(1)} all-to-all(bf16[16,32,16,256]{3,2,1,0:T(8,128)(2,1)S(1)} %stack.5), channel_id=1, replica_groups=mesh['sp_0'=16,'sp_1'=2,'tp_0'=4,'tp_1'=4] {'tp_0','tp_1'}, dimensions={0} | all-to-all | bytes 8388608 | tf_op jit(solution)/shard_map/all_to_all | solution.py:220
  284.7 1.2 fusion.23
  286.0 1.3 fusion.6
  287.7 30.3 %all_to_all.27 = bf16[16,32,16,128]{3,2,1,0:T(8,128)(2,1)S(1)} all-to-all(bf16[16,32,16,128]{3,2,1,0:T(8,128)(2,1)S(1)} %broadcast_in_dim.19), channel_id=1, replica_groups=mesh['sp_0'=16,'sp_1'=2,'tp_0'=4,'tp_1'=4] {'tp_0','tp_1'}, dimensions={0} | all-to-all | bytes 4194304 | tf_op jit(solution)/shard_map/all_to_all | solution.py:62
  318.0 1.4 fusion.3
  319.4 7.2 %all-to-all-start.4 = ((bf16[32,16,256]{2,1,0:T(8,128)(2,1)}), bf16[32,16,256]{2,1,0:T(8,128)(2,1)S(1)}, u32[]{:S(2)}, u32[]{:S(2)}) async-start(bf16[32,16,256]{2,1,0:T(8,128)(2,1)} %fusion.3), calls=%async_computation.4 | async-start | bytes 524288 | tf_op jit(solution)/shard_map/all_to_all | solution.py:233
  326.8 22.1 %all-to-all-done.4 = bf16[32,16,256]{2,1,0:T(8,128)(2,1)S(1)} async-done(((bf16[32,16,256]{2,1,0:T(8,128)(2,1)}), bf16[32,16,256]{2,1,0:T(8,128)(2,1)S(1)}, u32[]{:S(2)}, u32[]{:S(2)}) %all-to-all-start.4) | async-done | bytes 262176 | tf_op jit(solution)/shard_map/all_to_all | solution.py:233
  349.1 0.8 fusion.9
  (85 shorter events, 15.1 us)
Async XLA Ops:
  6.5 311.4 %copy-start = (bf16[1,2048,256]{2,1,0:T(8,128)(2,1)S(1)}, bf16[1,2048,256]{2,1,0:T(8,128)(2,1)}, u32[]{:S(2)}) copy-start(bf16[1,2048,256]{2,1,0:T(8,128)(2,1)} %param.31) | copy-start | bytes 3145732
  6.5 26.8 %copy-start.2 = (bf16[128,2,128]{2,1,0:T(2,128)(2,1)S(1)}, bf16[128,2,128]{2,1,0:T(2,128)(2,1)}, u32[]{:S(2)}) copy-start(bf16[128,2,128]{2,1,0:T(2,128)(2,1)} %param.22) | copy-start | bytes 196612
  6.5 27.5 %copy-start.6 = (f32[2,128]{1,0:T(2,128)S(1)}, f32[2,128]{1,0:T(2,128)}, u32[]{:S(2)}) copy-start(f32[2,128]{1,0:T(2,128)} %param.24) | copy-start | bytes 3076
  6.5 90.4 %all-gather.9.cloned.1.call-start = ((), (), s32[]{:S(2)}) async-start(), calls=%async_computation.6 | async-start | bytes 3411968 | tf_op jit(solution)/shard_map/all_gather | solution.py:30
  31.2 145.7 %all-gather.7.cloned.1.call-start = ((), (), s32[]{:S(2)}) async-start(), calls=%async_computation.5 | async-start | bytes 2162688 | tf_op jit(solution)/shard_map/all_gather | solution.py:195
  112.3 20.5 %copy-start.4 = (s32[128,2]{0,1:T(2,128)S(1)}, s32[128,2]{0,1:T(2,128)}, u32[]{:S(2)}) copy-start(s32[128,2]{0,1:T(2,128)} %param.27) | copy-start | bytes 3076
  112.3 64.6 %copy-start.3 = (bf16[128,256]{1,0:T(8,128)(2,1)S(1)}, bf16[128,256]{1,0:T(8,128)(2,1)}, u32[]{:S(2)}) copy-start(bf16[128,256]{1,0:T(8,128)(2,1)} %param.16) | copy-start | bytes 196612
  126.1 69.7 %copy-start.5 = (f32[256]{0:T(256)S(1)}, f32[256]{0:T(256)}, u32[]{:S(2)}) copy-start(f32[256]{0:T(256)} %param.26) | copy-start | bytes 3076
  126.1 50.8 %all-to-all-start = ((bf16[16,128,2,128]{3,1,2,0:T(8,128)(2,1)}), bf16[16,128,2,128]{3,1,2,0:T(8,128)(2,1)S(1)}, u32[]{:S(2)}, u32[]{:S(2)}) async-start(bf16[16,128,2,128]{3,1,2,0:T(8,128)(2,1)} %broadcast_in_dim.18), calls=%async_computation | async-start | bytes 2097152 | tf_op jit(solution)/shard_map/all_to_all | solution.py:62
  283.5 1.2 copy-start.1
  284.1 1.9 copy-start.8
  318.0 8.7 %copy-start.7 = (f32[128,2]{0,1:T(2,128)S(1)}, f32[128,2]{0,1:T(2,128)}, u32[]{:S(2)}) copy-start(f32[128,2]{0,1:T(2,128)} %param.28) | copy-start | bytes 3076
  319.4 29.5 %all-to-all-start.4 = ((bf16[32,16,256]{2,1,0:T(8,128)(2,1)}), bf16[32,16,256]{2,1,0:T(8,128)(2,1)S(1)}, u32[]{:S(2)}, u32[]{:S(2)}) async-start(bf16[32,16,256]{2,1,0:T(8,128)(2,1)} %fusion.3), calls=%async_computation.4 | async-start | bytes 524288 | tf_op jit(solution)/shard_map/all_to_all | solution.py:233
Sparse Core Ops, SparseCore 0:
  31.3 65.5 all-gather.8
  99.0 77.8 all-gather.6
